TPU v7x, 512 devices: a whole 4x4x16 slice. The times are simulated.
512 devices in a mesh: ep: 128 (over z, x, core), tp: 4 (over y).
Axes of the slice: x: 4, y: 4, z: 16, core: 2. Of those that a mesh axis runs over, the one named last changes fastest.
Arguments:
- tokens: bfloat16 [16384, 2048], P('ep'), may hold values from -6 to 6
- norm_gain: float32 [2048], replicated, may hold values from 0.1 to 1.9
- expert_ids: int32 [16384, 2], P('ep'), may hold values from 0 to 31, all different within a row; in each aligned block of 128 rows (0 to 127, 128 to 255, ...) at most 12 rows name the same one
- gate_weights: float32 [16384, 2], P('ep'), may hold values from 0.2 to 1
- w_gate: bfloat16 [2048, 131072], P(None, ('ep', 'tp')), may hold values from -0.125 to 0.125
- w_up: bfloat16 [2048, 131072], P(None, ('ep', 'tp')), may hold values from -0.125 to 0.125
- w_down: bfloat16 [131072, 2048], P('ep', 'tp'), may hold values from -0.09375 to 0.09375
Outputs:
- moe_out: bfloat16 [16384, 2048], P('ep', 'tp')
Inputs may be any that keep to these rules, and one draw needn't show every extreme that they name: `expert_ids`: each token names 2 different experts; in each aligned block of 128 rows no expert is named by more than 12 rows, a bound that some block reaches.
All inputs are finite; a program needn't handle non-finite values.
Results may differ from a plain program's by a relative error of at most 0.0071.
Values may be sent and summed in bfloat16 or wider, within the bound.
No kernel may reach another device: no remote copies, remote signals or barrier semaphores. Data moves between devices by JAX's collectives and lax.ppermute only.
A program may use at most 64 MiB of HBM per device.

v0:
```python
import jax
import jax.numpy as jnp
from jax import lax
from jax.sharding import Mesh
from jax.sharding import PartitionSpec as P

TOP = 2
EP = ("ep_0", "ep_1", "ep_2")
EP_TP = ("ep_0", "ep_1", "ep_2", "tp")
EPS = 1e-06


def split_up(array, dim, length):
    lengths = array.shape
    parts = array.reshape(*lengths[:dim], length, lengths[dim] // length, *lengths[dim + 1 :])
    return jnp.moveaxis(parts, dim, 0)


def laid_out(parts, dim):
    parts = jnp.moveaxis(parts, 0, dim)
    lengths = parts.shape
    return parts.reshape(*lengths[:dim], lengths[dim] * lengths[dim + 1], *lengths[dim + 2 :])


def turned_blocks(parts, axes, sequence):
    inside = parts.shape[1:]
    out = parts.reshape(*(lax.axis_size(a) for a in axes), *inside)
    for k in sequence:
        out = lax.all_to_all(out, axes[k], k, k, tiled=True)
    return out.reshape(-1, *inside)


def exchange_by_chip(array, groups, sequence, split_dim, concat_dim):
    length = lax.axis_size(groups[0]) * lax.axis_size(groups[1])
    parts = split_up(array, split_dim, length)
    return laid_out(turned_blocks(parts, groups, sequence), concat_dim)


def rms_rows(values, gain):
    widened = values.astype(jnp.float32)
    scale = lax.rsqrt(jnp.mean(widened * widened, axis=-1, keepdims=True) + EPS)
    return (widened * scale * gain).astype(jnp.bfloat16)


def on_device(tokens, norm_gain, expert_ids, gate_weights, w_gate, w_up, w_down):
    ep_count = lax.axis_size(EP)
    tp_count = lax.axis_size("tp")
    row_count = tokens.shape[0]
    group_size = max(1, ep_count // 32)
    expert_count = ep_count // group_size
    share = (row_count * TOP * 5 + 4 * expert_count * tp_count - 1) // (4 * expert_count * tp_count)
    capacity = min(row_count, tp_count * share)
    normed = rms_rows(tokens, norm_gain)
    flat_ids = expert_ids.reshape(-1)
    matches = (flat_ids[:, None] == jnp.arange(expert_count, dtype=jnp.int32)[None, :]).astype(
        jnp.int32
    )
    slot_index = jnp.sum((jnp.cumsum(matches, axis=0) - matches) * matches, axis=1)
    position = flat_ids * capacity + slot_index
    placing = (
        position[:, None] == jnp.arange(expert_count * capacity, dtype=jnp.int32)[None, :]
    ).astype(jnp.float32)
    placing = placing.reshape(row_count, TOP, expert_count * capacity)
    selector = jnp.sum(placing, axis=1).astype(jnp.bfloat16)
    buffers = lax.dot_general(
        selector, normed, (((0,), (0,)), ((), ())), preferred_element_type=jnp.float32
    )
    buffers = buffers.astype(jnp.bfloat16).reshape(expert_count, capacity, -1)
    quarter = capacity // tp_count
    mine = lax.dynamic_slice_in_dim(buffers, lax.axis_index("tp") * quarter, quarter, 1)
    copies = jnp.repeat(mine, group_size, axis=0)
    arrived = exchange_by_chip(copies, (("ep_0", "ep_1"), "ep_2"), (1, 0), 0, 0)
    received = lax.all_gather(arrived, "tp", axis=1, tiled=True)
    sources, slot_count, model_width = received.shape
    flat_rows = received.reshape(sources * slot_count, model_width)
    gate_proj = jnp.dot(flat_rows, w_gate, preferred_element_type=jnp.float32)
    upper = jnp.dot(flat_rows, w_up, preferred_element_type=jnp.float32)
    hidden = (jax.nn.silu(gate_proj) * upper).astype(jnp.bfloat16)
    partial_out = jnp.dot(
        lax.all_gather(hidden, "tp", axis=1, tiled=True), w_down, preferred_element_type=jnp.float32
    ).astype(jnp.bfloat16)
    partial_out = partial_out.reshape(sources, slot_count, w_down.shape[1])
    sources, slot_count, out_width = partial_out.shape
    back = exchange_by_chip(partial_out, (("ep_0", "ep_1"), "ep_2"), (1, 0), 0, 0)
    back = back.reshape(expert_count, group_size, slot_count, out_width).astype(jnp.float32)
    returned = jnp.sum(back, axis=1)
    summed = returned.reshape(expert_count * capacity, -1)
    combine = jnp.sum(placing * gate_weights[:, :, None], axis=1)
    mixed = jnp.dot(
        combine, summed, precision=lax.Precision.HIGHEST, preferred_element_type=jnp.float32
    )
    return mixed.astype(jnp.bfloat16)


def solution(mesh):
    finer = Mesh(mesh.devices.reshape(16, 4, 2, mesh.shape["tp"]), ("ep_0", "ep_1", "ep_2", "tp"))
    placed = (
        P(EP, None),
        P(),
        P(EP, None),
        P(EP, None),
        P(None, EP_TP),
        P(None, EP_TP),
        P(EP, "tp"),
    )
    return jax.shard_map(
        on_device, mesh=finer, in_specs=placed, out_specs=P(EP, "tp"), check_vma=False
    )
```

profile of v0, /device:TPU:2, one launch (start us, length us, event | category | flops | bytes accessed | tf_op | source)
XLA Modules:
  0.0 389.9 jit_solution(7729169001689056819)
XLA Ops:
  6.5 0.9 copy.81
  7.7 1.2 fusion.1
  9.0 0.6 reduce-window.6
  10.1 0.7 multiply_add_fusion
  10.8 0.8 convert_reduce_fusion.1
  11.7 1.4 convolution_convert_fusion.1
  13.1 1.5 reshape.57
  14.6 2.0 constant_dynamic-slice_fusion
  16.6 0.3 copy.85
  16.9 0.5 broadcast_in_dim.6
  17.4 0.3 broadcast_in_dim.14
  17.8 5.0 %all_to_all.20 = bf16[64,2,1,3,2048]{4,0,3,2,1:T(8,128)(2,1)S(1)} all-to-all(bf16[64,2,1,3,2048]{4,0,3,2,1:T(8,128)(2,1)S(1)} %broadcast_in_dim.15), channel_id=1, replica_groups=mesh['ep_0'=16,'ep_1'=4,'ep_2'=2,'tp'=4] {'ep_2'}, dimensions={1} | all-to-all | bytes 3145728 | tf_op jit(solution)/shard_map/all_to_all | solution.py:29
  22.8 1.6 copy.86
  24.5 96.4 %all_to_all.21 = bf16[64,2,1,3,2048]{4,1,3,2,0:T(2,128)(2,1)S(1)} all-to-all(bf16[64,2,1,3,2048]{4,1,3,2,0:T(2,128)(2,1)S(1)} %copy.86), channel_id=1, replica_groups=mesh['ep_0'=16,'ep_1'=4,'ep_2'=2,'tp'=4] {'ep_0','ep_1'}, dimensions={0} | all-to-all | bytes 3145728 | tf_op jit(solution)/shard_map/all_to_all | solution.py:29
  120.8 1.1 copy.87
  122.0 2.0 reshape_reshape.3
  124.0 0.2 all-gather.5.cloned.1.call-start
  124.3 65.0 %all-gather.3.cloned.1.call-done = bf16[128,12,2048]{2,0,1:T(8,128)(2,1)} async-done(((bf16[128,3,2048]{2,0,1:T(8,128)(2,1)}), bf16[128,12,2048]{2,0,1:T(8,128)(2,1)}) %all-gather.3.cloned.1.call-update) | async-done | bytes 6291472 | tf_op jit(solution)/shard_map/all_gather | solution.py:73
  189.3 9.7 %copy.88 = bf16[128,12,2048]{2,1,0:T(8,128)(2,1)} copy(bf16[128,12,2048]{2,0,1:T(8,128)(2,1)} %all-gather.3.cloned.1.call-done) | data formatting | bytes 12582912 | tf_op jit(solution)/shard_map/all_gather | solution.py:73
  198.9 10.8 %reshape.58 = bf16[1536,2048]{1,0:T(8,128)(2,1)} reshape(bf16[128,12,2048]{2,1,0:T(8,128)(2,1)} %copy.88) | data formatting | bytes 12582912 | tf_op jit(solution)/shard_map/reshape | solution.py:75
  209.7 4.8 %fusion.12 = f32[1536,256]{1,0:T(8,128)S(1)} fusion(bf16[1536,2048]{1,0:T(8,128)(2,1)} %reshape.58, bf16[2048,256]{1,0:T(8,128)(2,1)S(1)} %copy-done.3), kind=kOutput, calls=%fused_computation.30 | convolution fusion | flops 1610612736 | bytes 8912896 | tf_op jit(solution)/shard_map/dot_general | solution.py:76
  214.6 3.0 fusion
  217.6 51.2 %all-gather.5.cloned.1.call-done = bf16[1536,1024]{1,0:T(8,128)(2,1)} async-done(((bf16[1536,256]{1,0:T(8,128)(2,1)}), bf16[1536,1024]{1,0:T(8,128)(2,1)}) %all-gather.5.cloned.1.call-update) | async-done | bytes 3145744 | tf_op jit(solution)/shard_map/all_gather | solution.py:80
  268.8 4.8 %convolution_convert_fusion = bf16[1536,512]{1,0:T(8,128)(2,1)} fusion(bf16[1536,1024]{1,0:T(8,128)(2,1)} %all-gather.5.cloned.1.call-done, bf16[1024,512]{1,0:T(8,128)(2,1)S(1)} %copy-done), kind=kOutput, calls=%fused_computation.1 | convolution fusion | flops 1611399168 | bytes 5767168 | tf_op jit(solution)/shard_map/dot_general | solution.py:79
  273.6 2.4 reshape_reshape_reshape.2
  276.0 0.9 copy.89
  276.8 5.0 %all_to_all.22 = bf16[64,2,1,12,512]{4,0,3,2,1:T(8,128)(2,1)S(1)} all-to-all(bf16[64,2,1,12,512]{4,0,3,2,1:T(8,128)(2,1)S(1)} %copy.89), channel_id=1, replica_groups=mesh['ep_0'=16,'ep_1'=4,'ep_2'=2,'tp'=4] {'ep_2'}, dimensions={1} | all-to-all | bytes 3145728 | tf_op jit(solution)/shard_map/all_to_all | solution.py:29
  281.8 1.6 copy.90
  283.5 93.7 %all_to_all.23 = bf16[64,2,1,12,512]{4,1,3,2,0:T(2,128)(2,1)S(1)} all-to-all(bf16[64,2,1,12,512]{4,1,3,2,0:T(2,128)(2,1)S(1)} %copy.90), channel_id=1, replica_groups=mesh['ep_0'=16,'ep_1'=4,'ep_2'=2,'tp'=4] {'ep_0','ep_1'}, dimensions={0} | all-to-all | bytes 3145728 | tf_op jit(solution)/shard_map/all_to_all | solution.py:29
  377.1 4.2 %convert_reduce_fusion = f32[64,12,512]{2,1,0:T(8,128)S(1)} fusion(bf16[64,2,1,12,512]{4,1,3,2,0:T(2,128)(2,1)S(1)} %all_to_all.23), kind=kLoop, calls=%fused_computation | loop fusion | flops 1179648 | bytes 3145728 | tf_op jit(solution)/shard_map/reduce_sum | solution.py:86
  381.4 0.3 bitcast_reduce_fusion
  381.7 1.3 convolution_convert_fusion.2
  (25 shorter events, 1.2 us)
Async XLA Ops:
  6.5 262.3 %copy-start = (bf16[1024,512]{1,0:T(8,128)(2,1)S(1)}, bf16[1024,512]{1,0:T(8,128)(2,1)}, u32[]{:S(2)}) copy-start(bf16[1024,512]{1,0:T(8,128)(2,1)} %param.13) | copy-start | bytes 3145732
  6.5 5.1 %copy-start.2 = (bf16[128,2048]{1,0:T(8,128)(2,1)S(1)}, bf16[128,2048]{1,0:T(8,128)(2,1)}, u32[]{:S(2)}) copy-start(bf16[128,2048]{1,0:T(8,128)(2,1)} %param.7) | copy-start | bytes 1572868
  6.5 182.7 %all-gather.3.cloned.1.call-start = ((), (), s32[]{:S(2)}) async-start(), calls=%async_computation.4 | async-start | bytes 7864320 | tf_op jit(solution)/shard_map/all_gather | solution.py:73
  124.0 144.7 %all-gather.5.cloned.1.call-start = ((), (), s32[]{:S(2)}) async-start(), calls=%async_computation.5 | async-start | bytes 3932160 | tf_op jit(solution)/shard_map/all_gather | solution.py:80
  198.9 10.8 %copy-start.3 = (bf16[2048,256]{1,0:T(8,128)(2,1)S(1)}, bf16[2048,256]{1,0:T(8,128)(2,1)}, u32[]{:S(2)}) copy-start(bf16[2048,256]{1,0:T(8,128)(2,1)} %param.11) | copy-start | bytes 3145732
  209.7 4.8 %copy-start.1 = (bf16[1536,2048]{1,0:T(8,128)(2,1)S(1)}, bf16[1536,2048]{1,0:T(8,128)(2,1)}, u32[]{:S(2)}) copy-start(bf16[1536,2048]{1,0:T(8,128)(2,1)} %reshape.58) | copy-start | bytes 18874372
  209.7 4.9 %copy-start.4 = (bf16[2048,256]{1,0:T(8,128)(2,1)S(1)}, bf16[2048,256]{1,0:T(8,128)(2,1)}, u32[]{:S(2)}) copy-start(bf16[2048,256]{1,0:T(8,128)(2,1)} %param.12) | copy-start | bytes 3145732
Sparse Core Ops, SparseCore 0:
  124.2 65.0 all-gather.2
  217.7 51.0 all-gather.4
where the time goes:
time: 391 us; the launch traced here: 390 us
  blocking collectives  200 us (51%)
  waiting for transfers between devices  116 us (30%)
  local copies, waits for them, and re-layouts  36.5 us (9%)
  matrix products  15.2 us (4%)
  between operations  13.6 us (3%)
  other arithmetic  8.01 us (2%)
    all_to_all x4, blocking collectives, turned_blocks(): out = lax.all_to_all(out, axes[k], k, k, tiled=True)  200 us
    all_gather x1, waiting for transfers between devices, on_device(): received = lax.all_gather(arrived, 'tp', axis=1, tiled=True)  65 us
    all_gather x1, waiting for transfers between devices, on_device(): lax.all_gather(hidden, 'tp', axis=1, tiled=True)  51.2 us
    reshape x1, local copies, waits for them, and re-layouts, on_device(): flat_rows = received.reshape(sources * slot_count, model_width)  10.8 us
    all_gather x1, local copies, waits for them, and re-layouts, on_device(): received = lax.all_gather(arrived, 'tp', axis=1, tiled=True)  9.65 us
  transfers between devices with their start and end apart: 2, of which 2 were waited for; matrix products, arithmetic and copies ran while one was open for 0% of the time, Pallas kernels for 0%

commit v1 on v0

--- a/solution.py
+++ b/solution.py
@@ -70,7 +70,8 @@
     mine = lax.dynamic_slice_in_dim(buffers, lax.axis_index("tp") * quarter, quarter, 1)
     copies = jnp.repeat(mine, group_size, axis=0)
     arrived = exchange_by_chip(copies, (("ep_0", "ep_1"), "ep_2"), (1, 0), 0, 0)
-    received = lax.all_gather(arrived, "tp", axis=1, tiled=True)
+    copies_2 = jnp.concatenate([arrived] * lax.axis_size("tp"), axis=1)
+    received = lax.all_to_all(copies_2, "tp", 1, 1, tiled=True)
     sources, slot_count, model_width = received.shape
     flat_rows = received.reshape(sources * slot_count, model_width)
     gate_proj = jnp.dot(flat_rows, w_gate, preferred_element_type=jnp.float32)

time: 391 us -> 391 us (level)
  waiting for transfers between devices: 116 us -> 42.7 us
  blocking collectives: 200 us -> 273 us
  other arithmetic: 8.01 us -> 12.3 us
    all_to_all x0 -> x1, blocking collectives: none -> 72.9 us  [on_device(): received = lax.all_to_all(copies_2, 'tp', 1, 1, tiled=True)]
    all_gather x1 -> x0, waiting for transfers between devices: 65 us -> none  [on_device(): received = lax.all_gather(arrived, 'tp', axis=1, tiled=True)]
    all_gather x1 -> x0, local copies, waits for them, and re-layouts: 9.65 us -> none  [on_device(): received = lax.all_gather(arrived, 'tp', axis=1, tiled=True)]
    all_gather x1, waiting for transfers between devices: 51.2 us -> 42.6 us  [on_device(): lax.all_gather(hidden, 'tp', axis=1, tiled=True)]
    all_to_all x0 -> x1, local copies, waits for them, and re-layouts: none -> 6.85 us  [on_device(): received = lax.all_to_all(copies_2, 'tp', 1, 1, tiled=True)]
    concatenate x0 -> x1, other arithmetic: none -> 4.25 us  [on_device(): copies_2 = jnp.concatenate([arrived] * lax.axis_size('tp'), axis=1)]
  transfers between devices with their start and end apart: 2 -> 1, of which waited for: 2 -> 1; matrix products, arithmetic and copies ran while one was open for 0% -> 0% of each run, Pallas kernels for 0% -> 0%
where the time goes in v1:
time: 391 us
  blocking collectives  273 us (70%)
  waiting for transfers between devices  42.7 us (11%)
  local copies, waits for them, and re-layouts  33.7 us (9%)
  matrix products  15.6 us (4%)
  between operations  13.6 us (3%)
  other arithmetic  12.3 us (3%)
    all_to_all x4, blocking collectives, turned_blocks(): out = lax.all_to_all(out, axes[k], k, k, tiled=True)  200 us
    all_to_all x1, blocking collectives, on_device(): received = lax.all_to_all(copies_2, 'tp', 1, 1, tiled=True)  72.9 us
    all_gather x1, waiting for transfers between devices, on_device(): lax.all_gather(hidden, 'tp', axis=1, tiled=True)  42.6 us
    reshape x1, local copies, waits for them, and re-layouts, on_device(): flat_rows = received.reshape(sources * slot_count, model_width)  10.8 us
  transfers between devices with their start and end apart: 1, of which 1 were waited for; matrix products, arithmetic and copies ran while one was open for 0% of the time, Pallas kernels for 0%

profile of v1, /device:TPU:2, one launch (start us, length us, event | category | flops | bytes accessed | tf_op | source)
XLA Modules:
  0.0 390.6 jit_solution(8728948546626477701)
XLA Ops:
  6.5 0.9 copy.81
  7.7 1.2 fusion.1
  8.9 0.6 reduce-window.6
  10.1 0.7 multiply_add_fusion
  10.8 0.8 convert_reduce_fusion.1
  11.6 1.7 convolution_convert_fusion.1
  13.4 1.5 reshape.57
  14.9 2.0 constant_dynamic-slice_fusion
  16.9 0.3 copy.85
  17.2 0.5 broadcast_in_dim.6
  17.7 0.3 broadcast_in_dim.14
  18.1 5.0 %all_to_all.25 = bf16[64,2,1,3,2048]{4,0,3,2,1:T(8,128)(2,1)S(1)} all-to-all(bf16[64,2,1,3,2048]{4,0,3,2,1:T(8,128)(2,1)S(1)} %broadcast_in_dim.15), channel_id=1, replica_groups=mesh['ep_0'=16,'ep_1'=4,'ep_2'=2,'tp'=4] {'ep_2'}, dimensions={1} | all-to-all | bytes 3145728 | tf_op jit(solution)/shard_map/all_to_all | solution.py:29
  23.1 1.6 copy.86
  24.8 96.4 %all_to_all.26 = bf16[64,2,1,3,2048]{4,1,3,2,0:T(2,128)(2,1)S(1)} all-to-all(bf16[64,2,1,3,2048]{4,1,3,2,0:T(2,128)(2,1)S(1)} %copy.86), channel_id=1, replica_groups=mesh['ep_0'=16,'ep_1'=4,'ep_2'=2,'tp'=4] {'ep_0','ep_1'}, dimensions={0} | all-to-all | bytes 3145728 | tf_op jit(solution)/shard_map/all_to_all | solution.py:29
  121.2 1.1 copy.87
  122.3 2.0 reshape_reshape.3
  124.3 4.2 %pad_maximum_fusion = bf16[128,12,2048]{2,0,1:T(8,128)(2,1)S(1)} fusion(bf16[128,3,2048]{2,0,1:T(8,128)(2,1)} %reshape_reshape.3), kind=kLoop, calls=%fused_computation | loop fusion | flops 9437184 | bytes 7864320 | tf_op jit(solution)/shard_map/concatenate | solution.py:73
  128.6 72.9 %all_to_all.27 = bf16[128,12,2048]{2,0,1:T(8,128)(2,1)S(1)} all-to-all(bf16[128,12,2048]{2,0,1:T(8,128)(2,1)S(1)} %pad_maximum_fusion), channel_id=1, replica_groups=mesh['ep_0'=16,'ep_1'=4,'ep_2'=2,'tp'=4] {'tp'}, dimensions={1} | all-to-all | bytes 12582912 | tf_op jit(solution)/shard_map/all_to_all | solution.py:74
  201.4 6.9 %copy.88 = bf16[128,12,2048]{2,1,0:T(8,128)(2,1)} copy(bf16[128,12,2048]{2,0,1:T(8,128)(2,1)S(1)} %all_to_all.27) | data formatting | bytes 12582912 | tf_op jit(solution)/shard_map/all_to_all | solution.py:74
  208.3 10.8 %reshape.58 = bf16[1536,2048]{1,0:T(8,128)(2,1)} reshape(bf16[128,12,2048]{2,1,0:T(8,128)(2,1)} %copy.88) | data formatting | bytes 12582912 | tf_op jit(solution)/shard_map/reshape | solution.py:76
  219.1 4.8 %fusion.12 = f32[1536,256]{1,0:T(8,128)S(1)} fusion(bf16[1536,2048]{1,0:T(8,128)(2,1)} %reshape.58, bf16[2048,256]{1,0:T(8,128)(2,1)S(1)} %copy-done.2), kind=kOutput, calls=%fused_computation.31 | convolution fusion | flops 1610612736 | bytes 8912896 | tf_op jit(solution)/shard_map/dot_general | solution.py:77
  223.9 3.0 fusion
  226.9 42.6 %all-gather.2.cloned.1.call-done = bf16[1536,1024]{1,0:T(8,128)(2,1)} async-done(((bf16[1536,256]{1,0:T(8,128)(2,1)}), bf16[1536,1024]{1,0:T(8,128)(2,1)}) %all-gather.2.cloned.1.call-update) | async-done | bytes 3145744 | tf_op jit(solution)/shard_map/all_gather | solution.py:81
  269.5 4.8 %convolution_convert_fusion = bf16[1536,512]{1,0:T(8,128)(2,1)} fusion(bf16[1536,1024]{1,0:T(8,128)(2,1)} %all-gather.2.cloned.1.call-done, bf16[1024,512]{1,0:T(8,128)(2,1)S(1)} %copy-done), kind=kOutput, calls=%fused_computation.2 | convolution fusion | flops 1611399168 | bytes 5767168 | tf_op jit(solution)/shard_map/dot_general | solution.py:80
  274.4 2.4 reshape_reshape_reshape.2
  276.7 0.9 copy.89
  277.6 5.0 %all_to_all.28 = bf16[64,2,1,12,512]{4,0,3,2,1:T(8,128)(2,1)S(1)} all-to-all(bf16[64,2,1,12,512]{4,0,3,2,1:T(8,128)(2,1)S(1)} %copy.89), channel_id=1, replica_groups=mesh['ep_0'=16,'ep_1'=4,'ep_2'=2,'tp'=4] {'ep_2'}, dimensions={1} | all-to-all | bytes 3145728 | tf_op jit(solution)/shard_map/all_to_all | solution.py:29
  282.6 1.6 copy.90
  284.2 93.7 %all_to_all.29 = bf16[64,2,1,12,512]{4,1,3,2,0:T(2,128)(2,1)S(1)} all-to-all(bf16[64,2,1,12,512]{4,1,3,2,0:T(2,128)(2,1)S(1)} %copy.90), channel_id=1, replica_groups=mesh['ep_0'=16,'ep_1'=4,'ep_2'=2,'tp'=4] {'ep_0','ep_1'}, dimensions={0} | all-to-all | bytes 3145728 | tf_op jit(solution)/shard_map/all_to_all | solution.py:29
  377.9 4.2 %convert_reduce_fusion = f32[64,12,512]{2,1,0:T(8,128)S(1)} fusion(bf16[64,2,1,12,512]{4,1,3,2,0:T(2,128)(2,1)S(1)} %all_to_all.29), kind=kLoop, calls=%fused_computation.1 | loop fusion | flops 1179648 | bytes 3145728 | tf_op jit(solution)/shard_map/reduce_sum | solution.py:87
  382.1 0.3 bitcast_reduce_fusion
  382.5 1.3 convolution_convert_fusion.2
  (22 shorter events, 1.1 us)
Async XLA Ops:
  6.5 263.0 %copy-start = (bf16[1024,512]{1,0:T(8,128)(2,1)S(1)}, bf16[1024,512]{1,0:T(8,128)(2,1)}, u32[]{:S(2)}) copy-start(bf16[1024,512]{1,0:T(8,128)(2,1)} %param.13) | copy-start | bytes 3145732
  6.5 263.0 %all-gather.2.cloned.1.call-start = ((), (), s32[]{:S(2)}) async-start(), calls=%async_computation.5 | async-start | bytes 3932160 | tf_op jit(solution)/shard_map/all_gather | solution.py:81
  208.3 10.8 %copy-start.2 = (bf16[2048,256]{1,0:T(8,128)(2,1)S(1)}, bf16[2048,256]{1,0:T(8,128)(2,1)}, u32[]{:S(2)}) copy-start(bf16[2048,256]{1,0:T(8,128)(2,1)} %param.11) | copy-start | bytes 3145732
  219.1 4.8 %copy-start.1 = (bf16[1536,2048]{1,0:T(8,128)(2,1)S(1)}, bf16[1536,2048]{1,0:T(8,128)(2,1)}, u32[]{:S(2)}) copy-start(bf16[1536,2048]{1,0:T(8,128)(2,1)} %reshape.58) | copy-start | bytes 18874372
  219.1 4.9 %copy-start.3 = (bf16[2048,256]{1,0:T(8,128)(2,1)S(1)}, bf16[2048,256]{1,0:T(8,128)(2,1)}, u32[]{:S(2)}) copy-start(bf16[2048,256]{1,0:T(8,128)(2,1)} %param.12) | copy-start | bytes 3145732
Sparse Core Ops, SparseCore 0:
  227.0 42.4 all-gather.1
